TPU v7x, 32 devices: a whole 2x2x4 slice. The times are simulated.
32 devices in a mesh: fs: 8 (over z, x), tp: 4 (over y, core).
Axes of the slice: x: 2, y: 2, z: 4, core: 2. Of those that a mesh axis runs over, the one named last changes fastest.
Arguments:
- tokens: bfloat16 [768, 4, 2048], P(None, 'tp'), may hold values from -6 to 6
- norm_gain: float32 [2048], P('fs'), may hold values from 0.1 to 1.9
- gate_weight: float32 [8, 2048, 4096], P(None, 'fs', 'tp'), may hold values from -0.125 to 0.125
- up_weight: float32 [8, 2048, 4096], P(None, 'fs', 'tp'), may hold values from -0.125 to 0.125
- down_weight: float32 [8, 2048, 4096], P(None, 'fs', 'tp'), may hold values from -0.09375 to 0.09375
- expert_ids: int32 [768, 4, 2], P(None, 'tp'), may hold values from 0 to 7, all different within a row
- expert_mix: float32 [768, 4, 2], P(None, 'tp'), may hold values from 0.2 to 1
Outputs:
- gate_serve: bfloat16 [8, 2048, 4096], P(None, None, 'fs')
- up_serve: bfloat16 [8, 2048, 4096], P(None, None, 'fs')
- down_serve: bfloat16 [8, 2048, 4096], P(None, None, 'fs')
- mixed: bfloat16 [768, 4, 2048], P('fs', 'tp')
Inputs may be any that keep to these rules, and one draw needn't show every extreme that they name: `expert_ids`: each token names two different experts.
All inputs are finite; a program needn't handle non-finite values.
Results may differ from a plain program's by a relative error of at most 0.0082.
Values may be sent and summed in bfloat16 or wider, within the bound.
A program may use at most 192 MiB of HBM per device.

v0:
```python
import functools

import jax
import jax.numpy as jnp
from jax import lax
from jax.experimental import pallas as pl
from jax.experimental.pallas import tpu as pltpu
from jax.sharding import PartitionSpec as P

norm_eps = 1e-05
MESH = pl.DeviceIdType.MESH


PARTS = 2
LEAD = 4
LAG = 10
GAP = 2


def exchange_kernel(n_fs, n_tp, tokens, gain, ids, mix, gate_in, up_in, down_in, gate_out, up_out, down_out, relay_buf,
                    partial, cast, raw, normed, gates, held, total, hop_send, hop_recv, own_send, pass_send, core_send,
                    side_send, land, load, fetch):
    raws, outs = (gate_in, up_in, down_in), (gate_out, up_out, down_out)
    experts, rows, columns = gate_in.shape
    per = n_fs // n_tp
    unit = columns // per
    sub = rows // PARTS
    chunks = experts * PARTS
    half = n_fs // 2
    f, t = lax.axis_index("fs"), lax.axis_index("tp")
    mate = t + 1 - 2 * lax.rem(t, 2)
    side = lax.rem(t + 2, n_tp)
    own = lax.div(f, per)
    own_mate = own + 1 - 2 * lax.rem(own, 2)
    near = t == own_mate
    far = t == lax.rem(own_mate + 2, n_tp)
    inner = lax.div(f, half) == lax.div(t, 2)
    cross = pl.ds((1 - lax.div(f, half)) * half, half)

    def place(j):
        return lax.div(j, PARTS), pl.ds(pl.multiple_of(lax.rem(j, PARTS) * sub, sub), sub)

    def hop(k, j):
        e, now = place(j)
        return pltpu.make_async_remote_copy(
            src_ref=cast.at[k, e, now], dst_ref=relay_buf.at[k - 1, e, now], send_sem=hop_send.at[k - 1, j],
            recv_sem=hop_recv.at[k - 1, j], device_id=(f, side), device_id_type=MESH)

    def straight(k, j, h):
        e, now = place(j)
        return pltpu.make_async_remote_copy(
            src_ref=cast.at[k, e, now, pl.ds(h * unit, unit)], dst_ref=outs[k].at[e, f, now],
            send_sem=own_send.at[k, j, h], recv_sem=land.at[k, j], device_id=(t * per + h, mate), device_id_type=MESH)

    def relayed(k, j, h):
        e, now = place(j)
        return pltpu.make_async_remote_copy(
            src_ref=relay_buf.at[k - 1, e, now, pl.ds(h * unit, unit)], dst_ref=outs[k].at[e, f, now],
            send_sem=pass_send.at[k - 1, j, h], recv_sem=land.at[k, j],
            device_id=(side * per + h, mate), device_id_type=MESH)

    def to_mate(k, j):
        e, now = place(j)
        return pltpu.make_async_remote_copy(
            src_ref=outs[k].at[e, :, now], dst_ref=outs[k].at[e, :, now], send_sem=core_send.at[k, j],
            recv_sem=land.at[k, j], device_id=(f, mate), device_id_type=MESH)

    def to_side(k, j):
        e, now = place(j)
        which = cross if k == 2 else slice(None)
        return pltpu.make_async_remote_copy(
            src_ref=outs[k].at[e, which, now], dst_ref=outs[k].at[e, which, now], send_sem=side_send.at[k, j],
            recv_sem=land.at[k, j], device_id=(f, side), device_id_type=MESH)

    def landed(k, j):
        to_mate(k, j).wait_recv()

    def reads(j, slot):
        e, now = place(j)
        return [pltpu.make_async_copy(raws[k].at[e, now], raw.at[slot, k], fetch.at[slot, k]) for k in range(3)]

    def rounded(j):
        slot = lax.rem(j, 2)
        e, now = place(j)

        @pl.when(j + 1 < chunks)
        def _():
            for copy in reads(j + 1, 1 - slot):
                copy.start()

        for copy in reads(j, slot):
            copy.wait()
        scale = gain[now, :]
        cast[2, e, now, :] = raw[slot, 2].astype(jnp.bfloat16)
        cast[1, e, now, :] = (raw[slot, 1] * scale).astype(jnp.bfloat16)
        cast[0, e, now, :] = (raw[slot, 0] * scale).astype(jnp.bfloat16)

    def sent(j):
        hop(2, j).start()
        hop(1, j).start()
        for k in (0, 1):
            for h in range(per):
                straight(k, j, h).start()

        @pl.when(inner)
        def _():
            for h in range(per):
                straight(2, j, h).start()

    def opened(j):
        @pl.when(j < chunks)
        def _():
            rounded(j)

        @pl.when((j >= 1) & (j < chunks + 1))
        def _():
            sent(j - 1)

    def loads(j):
        e, now = place(j)
        return [pltpu.make_async_copy(outs[k].at[e, :, now], held.at[k, :, now], load.at[k, lax.rem(j, PARTS)])
                for k in range(3)]

    tall = normed.shape[0] // 2
    deep = n_fs * rows

    def compute(e):
        for r in range(PARTS):
            for copy in loads(e * PARTS + r):
                copy.wait()

        def some_rows(i, carry):
            now = pl.ds(pl.multiple_of(i * tall, tall), tall)
            fed = normed[now, :]
            gate_act = jnp.dot(fed, held[0].reshape(deep, unit), preferred_element_type=jnp.float32)
            up_act = jnp.dot(fed, held[1].reshape(deep, unit), preferred_element_type=jnp.float32)
            lanes = lax.broadcasted_iota(jnp.int32, (tall, gates.shape[1]), 1)
            gate = jnp.sum(jnp.where(lanes == e, gates[now, :], 0.0), axis=1, keepdims=True)
            hidden = gate_act / (1.0 + jnp.exp(-gate_act)) * up_act * gate
            total[now, :] += lax.dot_general(
                hidden.astype(jnp.bfloat16), held[2].reshape(deep, unit), (((1,), (1,)), ((), ())),
                preferred_element_type=jnp.float32)
            return carry

        lax.fori_loop(0, 2, some_rows, 0)

    for copy in reads(0, 0):
        copy.start()

    def early(j, carry):
        opened(j)
        return carry

    lax.fori_loop(0, LEAD + 1, early, 0)

    fair = normed.shape[0] // 8

    def norm_rows(i):
        now = pl.ds(pl.multiple_of(i * fair, fair), fair)
        values = tokens[now, :].astype(jnp.float32)
        centered = values - jnp.mean(values, axis=1, keepdims=True)
        variance = jnp.mean(centered * centered, axis=1, keepdims=True)
        normed[now, :] = (centered * lax.rsqrt(variance + norm_eps)).astype(jnp.bfloat16)
        total[now, :] = jnp.zeros((fair, total.shape[1]), jnp.float32)

    expert = lax.broadcasted_iota(jnp.int32, (128, ids.shape[1]), 0)
    chosen = sum(jnp.where(ids[c:c + 1, :] == expert, mix[c:c + 1, :], 0.0) for c in range(2))
    gates[...] = chosen.T

    def step(s, carry):
        opened(s + LEAD + 1)

        @pl.when(s < chunks)
        def _():
            for k in (2, 1):
                hop(k, s).wait_recv()
                for h in range(per):
                    relayed(k, s, h).start()

        @pl.when(s < 8)
        def _():
            norm_rows(s)

        @pl.when((s >= LAG) & (s < chunks + LAG))
        def _():
            j = s - LAG

            @pl.when(near)
            def _():
                landed(0, j)
                to_side(0, j).start()
                to_mate(0, j).start()
                landed(1, j)
                to_mate(1, j).start()

            @pl.when(far)
            def _():
                landed(2, j)
                to_side(2, j).start()
                to_mate(2, j).start()
                landed(1, j)
                to_mate(1, j).start()

        @pl.when(s >= LAG + GAP)
        def _():
            j = s - LAG - GAP

            @pl.when(near)
            def _():
                landed(2, j)
                to_mate(2, j).start()

            @pl.when(far)
            def _():
                landed(0, j)
                to_mate(0, j).start()

            @pl.when(jnp.logical_not(near | far))
            def _():
                for k in range(3):
                    landed(k, j)

            for copy in loads(j):
                copy.start()

            @pl.when(lax.rem(j, PARTS) == PARTS - 1)
            def _():
                compute(lax.div(j, PARTS))

        return carry

    lax.fori_loop(0, chunks + LAG + GAP, step, 0)
    partial[...] = total[...].astype(jnp.bfloat16)

    def drain(j, carry):
        for k in (1, 2):
            hop(k, j).wait_send()
            for h in range(per):
                relayed(k, j, h).wait_send()
        for k in (0, 1):
            for h in range(per):
                straight(k, j, h).wait_send()

        @pl.when(inner)
        def _():
            for h in range(per):
                straight(2, j, h).wait_send()

        @pl.when(near | far)
        def _():
            for k in range(3):
                to_mate(k, j).wait_send()

        @pl.when(near)
        def _():
            to_side(0, j).wait_send()

        @pl.when(far)
        def _():
            to_side(2, j).wait_send()

        return carry

    lax.fori_loop(0, chunks, drain, 0)


def exchange(n_fs, n_tp, tokens, gain, ids, mix, weights):
    experts, rows, columns = weights[0].shape
    per = n_fs // n_tp
    unit = columns // per
    count, width = tokens.shape
    chunks = experts * PARTS
    serve = jax.ShapeDtypeStruct((experts, n_fs, rows, unit), jnp.bfloat16)
    relay = jax.ShapeDtypeStruct((2, experts, rows, columns), jnp.bfloat16)
    dma = pltpu.SemaphoreType.DMA
    outs = pl.pallas_call(
        functools.partial(exchange_kernel, n_fs, n_tp),
        out_shape=(serve, serve, serve, relay, jax.ShapeDtypeStruct(tokens.shape, jnp.bfloat16)),
        in_specs=[pl.BlockSpec(memory_space=pltpu.VMEM)] * 4 + [pl.BlockSpec(memory_space=pl.ANY)] * 3,
        out_specs=[pl.BlockSpec(memory_space=pl.ANY)] * 4 + [pl.BlockSpec(memory_space=pltpu.VMEM)],
        scratch_shapes=[
            pltpu.VMEM((3, experts, rows, columns), jnp.bfloat16),
            pltpu.VMEM((2, 3, rows // PARTS, columns), jnp.float32),
            pltpu.VMEM((count, width), jnp.bfloat16),
            pltpu.VMEM((count, 128), jnp.float32),
            pltpu.VMEM((3, n_fs, rows, unit), jnp.bfloat16),
            pltpu.VMEM((count, width), jnp.float32),
            dma((2, chunks)),
            dma((2, chunks)),
            dma((3, chunks, per)),
            dma((2, chunks, per)),
            dma((3, chunks)),
            dma((3, chunks)),
            dma((3, chunks)),
            dma((3, PARTS)),
            dma((2, 3)),
        ],
        compiler_params=pltpu.CompilerParams(has_side_effects=True, vmem_limit_bytes=60 * 1024 * 1024),
    )(tokens, gain, ids, mix, *weights)
    return tuple(out.reshape(experts, n_fs * rows, unit) for out in outs[:3]) + (outs[4],)


def copy_kernel(*refs):
    half = len(refs) // 2
    for source, target in zip(refs[:half], refs[half:]):
        target[...] = source[...]


def copied(arrays):
    experts, deep, unit = arrays[0].shape
    block = pl.BlockSpec((1, deep, unit), lambda e: (e, 0, 0))
    return pl.pallas_call(
        copy_kernel,
        grid=(experts,),
        out_shape=tuple(jax.ShapeDtypeStruct(a.shape, a.dtype) for a in arrays),
        in_specs=[block] * len(arrays),
        out_specs=[block] * len(arrays),
        cost_estimate=pl.CostEstimate(flops=0, bytes_accessed=4 * len(arrays) * arrays[0].size, transcendentals=0),
        compiler_params=pltpu.CompilerParams(vmem_limit_bytes=40 * 1024 * 1024),
    )(*arrays)


def collective_exchange(blocks):
    regrouped = [lax.all_to_all(b, "tp", split_axis=0, concat_axis=2, tiled=True) for b in blocks]
    unit_split = [lax.all_to_all(b, "fs", split_axis=2, concat_axis=1, tiled=True) for b in regrouped]
    return tuple(lax.all_gather(b, "tp", axis=0, tiled=True) for b in unit_split)


def expert_layer(normed, expert_gates, gate_serve, up_serve, down_serve):
    gate_act = jnp.einsum("rd,edf->ref", normed, gate_serve, preferred_element_type=jnp.float32)
    up_act = jnp.einsum("rd,edf->ref", normed, up_serve, preferred_element_type=jnp.float32)
    hidden = (jax.nn.silu(gate_act) * up_act * expert_gates[:, :, None]).astype(jnp.bfloat16)
    return jnp.einsum("ref,edf->rd", hidden, down_serve, preferred_element_type=jnp.float32).astype(jnp.bfloat16)


def sum_parts(parts, n_fs):
    if n_fs > 8:
        parts = lax.all_to_all(parts, "fs", split_axis=0, concat_axis=0, tiled=True)
        return jnp.sum(parts.astype(jnp.float32), axis=0)
    f = lax.axis_index("fs")
    got = [lax.dynamic_index_in_dim(parts, f, 0, keepdims=False)]
    for j in range(1, n_fs):
        mine = lax.dynamic_index_in_dim(parts, lax.rem(f + j, n_fs), 0, keepdims=False)
        got.append(lax.ppermute(mine, "fs", [(i, (i + j) % n_fs) for i in range(n_fs)]))
    return sum(g.astype(jnp.float32) for g in got)


def local(tokens, norm_gain, gate_weight, up_weight, down_weight, expert_ids, expert_mix):
    n_fs, n_tp = lax.axis_size("fs"), lax.axis_size("tp")
    width = tokens.shape[2]
    token_rows = tokens.reshape(-1, width)
    count = token_rows.shape[0]
    route_ids = expert_ids.reshape(-1, 2)
    route_mix = expert_mix.reshape(-1, 2)
    rows, columns = gate_weight.shape[1:]
    unit = columns * n_tp // n_fs
    whole = count % 128 == 0 and n_fs % 2 == 0 and rows % (16 * PARTS) == 0
    if n_tp == 4 and n_fs % n_tp == 0 and unit % 128 == 0 and whole:
        gate_serve, up_serve, down_serve, partial = exchange(
            n_fs, n_tp, token_rows, norm_gain[:, None], route_ids.T, route_mix.T, (gate_weight, up_weight, down_weight))
        gate_serve, up_serve, down_serve = copied((gate_serve, up_serve, down_serve))
    else:
        blocks = (
            (gate_weight * norm_gain[None, :, None]).astype(jnp.bfloat16),
            (up_weight * norm_gain[None, :, None]).astype(jnp.bfloat16),
            down_weight.astype(jnp.bfloat16),
        )
        values = token_rows.astype(jnp.float32)
        centered = values - jnp.mean(values, axis=1, keepdims=True)
        variance = jnp.mean(centered * centered, axis=1, keepdims=True)
        normed = (centered * lax.rsqrt(variance + norm_eps)).astype(jnp.bfloat16)
        expert_iota = jnp.arange(gate_weight.shape[0], dtype=jnp.int32)
        chosen = (route_ids[:, :, None] == expert_iota[None, None, :]).astype(jnp.float32)
        expert_gates = jnp.sum(chosen * route_mix[:, :, None], axis=1)
        gate_serve, up_serve, down_serve = collective_exchange(blocks)
        partial = expert_layer(normed, expert_gates, gate_serve, up_serve, down_serve)
    own_rows = count // n_fs
    summed = sum_parts(partial.reshape(n_fs, own_rows, width), n_fs)
    mixed = summed.astype(jnp.bfloat16).reshape(own_rows, 1, width)
    return (gate_serve, up_serve, down_serve, mixed)


def solution(mesh):
    return jax.shard_map(
        local,
        mesh=mesh,
        in_specs=(
            P(None, "tp", None),
            P("fs"),
            P(None, "fs", "tp"),
            P(None, "fs", "tp"),
            P(None, "fs", "tp"),
            P(None, "tp", None),
            P(None, "tp", None),
        ),
        out_specs=(
            P(None, None, "fs"),
            P(None, None, "fs"),
            P(None, None, "fs"),
            P("fs", "tp", None),
        ),
        check_vma=False,
    )
```

profile of v0, /device:TPU:24, one launch (start us, length us, event | category | flops | bytes accessed | tf_op | source)
XLA Modules:
  0.0 497.6 jit_solution(14947742263434259667)
XLA Ops:
  0.7 1.5 copy.11.gain
  2.1 396.3 %shard_map.102 = (bf16[8,8,256,512]{3,2,1,0:T(8,128)(2,1)}, bf16[8,8,256,512]{3,2,1,0:T(8,128)(2,1)}, bf16[8,8,256,512]{3,2,1,0:T(8,128)(2,1)}, bf16[2,8,256,1024]{3,2,1,0:T(8,128)(2,1)}, bf16[768,2048]{1,0:T(8,128)(2,1)}) custom-call(bf16[768,2048]{1,0:T(8,128)(2,1)} %bitcast.36, f32[256,1]{1,0:T(8,128)} %copy.11.gain, s32[2,768]{1,0:T(2,128)} %bitcast.37, ...), custom_call_target="tpu_custom_call" | custom-call | tf_op jit(solution)/shard_map/pallas_call | solution.py:276
  398.4 1.9 dynamic-slice_bitcast_fusion.6
  400.4 3.7 collective-permute-start
  404.0 1.5 collective-permute-start.1
  405.5 6.2 %collective-permute-start.2 = (bf16[96,2048]{1,0:T(8,128)(2,1)S(1)}, bf16[96,2048]{1,0:T(8,128)(2,1)S(1)}, u32[]{:S(2)}, u32[]{:S(2)}) collective-permute-start(bf16[96,2048]{1,0:T(8,128)(2,1)S(1)} %get-tuple-element.23), channel_id=1, source_target_pairs={{0,12},{4,16},{8,20},{12,24},{16,28},{20,0},{24,4},{28,8},{1,13},{... | collective-permute-start | bytes 1179656 | tf_op jit(solution)/shard_map/ppermute | solution.py:344
  411.7 0.0 collective-permute-start.3
  411.7 3.7 collective-permute-start.4
  415.4 4.1 collective-permute-done
  419.5 4.4 collective-permute-start.5
  424.0 0.0 collective-permute-done.1
  424.0 38.9 %collective-permute-start.6 = (bf16[96,2048]{1,0:T(8,128)(2,1)S(1)}, bf16[96,2048]{1,0:T(8,128)(2,1)}, u32[]{:S(2)}, u32[]{:S(2)}) collective-permute-start(bf16[96,2048]{1,0:T(8,128)(2,1)S(1)} %get-tuple-element.19), channel_id=1, source_target_pairs={{0,28},{4,0},{8,4},{12,8},{16,12},{20,16},{24,20},{28,24},{1,29},{... | collective-permute-start | bytes 1179656 | tf_op jit(solution)/shard_map/ppermute | solution.py:344
  462.9 32.0 %shard_map.103 = (bf16[8,2048,512]{2,1,0:T(8,128)(2,1)}, bf16[8,2048,512]{2,1,0:T(8,128)(2,1)}, bf16[8,2048,512]{2,1,0:T(8,128)(2,1)}) custom-call(bf16[8,2048,512]{2,1,0:T(8,128)(2,1)} %bitcast.31, bf16[8,2048,512]{2,1,0:T(8,128)(2,1)} %bitcast.32, bf16[8,2048,512]{2,1,0:T(8,128)(2,1)} %bitcast.33), custom_call_target="tpu_custom_call" | custom-call | bytes 100663296 | tf_op jit(solution)/shard_map/pallas_call | solution.py:312
  494.9 0.0 collective-permute-done.2
  494.9 0.0 collective-permute-done.3
  494.9 0.0 collective-permute-done.4
  494.9 0.0 collective-permute-done.5
  494.9 0.0 collective-permute-done.6
  495.0 2.6 fusion.7
Async XLA Ops:
  400.4 19.2 %collective-permute-start = (bf16[96,2048]{1,0:T(8,128)(2,1)S(1)}, bf16[96,2048]{1,0:T(8,128)(2,1)S(1)}, u32[]{:S(2)}, u32[]{:S(2)}) collective-permute-start(bf16[96,2048]{1,0:T(8,128)(2,1)S(1)} %get-tuple-element.18), channel_id=1, source_target_pairs={{0,4},{4,8},{8,12},{12,16},{16,20},{20,24},{24,28},{28,0},{1,5},{5... | collective-permute-start | bytes 1179656 | tf_op jit(solution)/shard_map/ppermute | solution.py:344
  404.0 19.9 %collective-permute-start.1 = (bf16[96,2048]{1,0:T(8,128)(2,1)S(1)}, bf16[96,2048]{1,0:T(8,128)(2,1)S(1)}, u32[]{:S(2)}, u32[]{:S(2)}) collective-permute-start(bf16[96,2048]{1,0:T(8,128)(2,1)S(1)} %get-tuple-element.24), channel_id=1, source_target_pairs={{0,8},{4,12},{8,16},{12,20},{16,24},{20,28},{24,0},{28,4},{1,9},{5... | collective-permute-start | bytes 1179656 | tf_op jit(solution)/shard_map/ppermute | solution.py:344
  405.5 89.4 %collective-permute-start.2 = (bf16[96,2048]{1,0:T(8,128)(2,1)S(1)}, bf16[96,2048]{1,0:T(8,128)(2,1)S(1)}, u32[]{:S(2)}, u32[]{:S(2)}) collective-permute-start(bf16[96,2048]{1,0:T(8,128)(2,1)S(1)} %get-tuple-element.23), channel_id=1, source_target_pairs={{0,12},{4,16},{8,20},{12,24},{16,28},{20,0},{24,4},{28,8},{1,13},{... | collective-permute-start | bytes 1179656 | tf_op jit(solution)/shard_map/ppermute | solution.py:344
  411.7 83.2 %collective-permute-start.3 = (bf16[96,2048]{1,0:T(8,128)(2,1)S(1)}, bf16[96,2048]{1,0:T(8,128)(2,1)S(1)}, u32[]{:S(2)}, u32[]{:S(2)}) collective-permute-start(bf16[96,2048]{1,0:T(8,128)(2,1)S(1)} %get-tuple-element.22), channel_id=1, source_target_pairs={{0,16},{4,20},{8,24},{12,28},{16,0},{20,4},{24,8},{28,12},{1,17},{... | collective-permute-start | bytes 1179656 | tf_op jit(solution)/shard_map/ppermute | solution.py:344
  411.7 83.2 %collective-permute-start.4 = (bf16[96,2048]{1,0:T(8,128)(2,1)S(1)}, bf16[96,2048]{1,0:T(8,128)(2,1)}, u32[]{:S(2)}, u32[]{:S(2)}) collective-permute-start(bf16[96,2048]{1,0:T(8,128)(2,1)S(1)} %get-tuple-element.21), channel_id=1, source_target_pairs={{0,20},{4,24},{8,28},{12,0},{16,4},{20,8},{24,12},{28,16},{1,21},{... | collective-permute-start | bytes 1179656 | tf_op jit(solution)/shard_map/ppermute | solution.py:344
  419.5 75.4 %collective-permute-start.5 = (bf16[96,2048]{1,0:T(8,128)(2,1)S(1)}, bf16[96,2048]{1,0:T(8,128)(2,1)}, u32[]{:S(2)}, u32[]{:S(2)}) collective-permute-start(bf16[96,2048]{1,0:T(8,128)(2,1)S(1)} %get-tuple-element.20), channel_id=1, source_target_pairs={{0,24},{4,28},{8,0},{12,4},{16,8},{20,12},{24,16},{28,20},{1,25},{... | collective-permute-start | bytes 1179656 | tf_op jit(solution)/shard_map/ppermute | solution.py:344
  424.0 71.0 %collective-permute-start.6 = (bf16[96,2048]{1,0:T(8,128)(2,1)S(1)}, bf16[96,2048]{1,0:T(8,128)(2,1)}, u32[]{:S(2)}, u32[]{:S(2)}) collective-permute-start(bf16[96,2048]{1,0:T(8,128)(2,1)S(1)} %get-tuple-element.19), channel_id=1, source_target_pairs={{0,28},{4,0},{8,4},{12,8},{16,12},{20,16},{24,20},{28,24},{1,29},{... | collective-permute-start | bytes 1179656 | tf_op jit(solution)/shard_map/ppermute | solution.py:344
where the time goes:
time: 498 us
  Pallas kernels  428 us (86%)
  starting transfers between devices  58.4 us (12%)
    pallas_call x1, Pallas kernels, exchange(): pl.pallas_call(functools.partial(exchange_kernel, n_fs, n_tp), out_shape=...  396 us
    ppermute x7, starting transfers between devices, sum_parts(): lax.ppermute(mine, 'fs', [(i, (i + j) % n_fs) for i in range(n_fs)])  58.4 us
    pallas_call x1, Pallas kernels, copied(): pl.pallas_call(copy_kernel, grid=(experts,), out_shape=tuple((jax.ShapeDt...  32 us
  transfers between devices with their start and end apart: 7, of which 1 were waited for; matrix products, arithmetic and copies ran while one was open for 0% of the time, Pallas kernels for 6%

commit v1 on v0

v1 whole, which is shorter than its diff:
```python
import functools

import jax
import jax.numpy as jnp
from jax import lax
from jax.experimental import pallas as pl
from jax.experimental.pallas import tpu as pltpu
from jax.sharding import PartitionSpec as P

norm_eps = 1e-05
MESH = pl.DeviceIdType.MESH


STRIPS = 8
LEAD = 2
LAG = 4
GAP = 1
NORM_STEPS = 4


def exchange_kernel(n_fs, n_tp, tokens, gain, ids, mix, gate_in, up_in, down_in, stage, relay_buf, *rest):
    zs = n_fs // 2
    sums, rest = rest[:zs], rest[zs:]
    (scale, cast, raw, raw_down, normed, gates, hid, held, held_down, strip_sum, leaving, staying, arriving,
     hop_send, hop_recv, own_send, pass_send, core_send, side_send, land, load, load_down, fetch, fetch_down,
     pair_send, pair_recv) = rest
    experts, rows, columns = gate_in.shape
    per = n_fs // n_tp
    unit = columns // per
    strip = rows // STRIPS
    chunks = experts + STRIPS
    half = n_fs // 2
    f, t = lax.axis_index("fs"), lax.axis_index("tp")
    mate = t + 1 - 2 * lax.rem(t, 2)
    side = lax.rem(t + 2, n_tp)
    own = lax.div(f, per)
    own_mate = own + 1 - 2 * lax.rem(own, 2)
    near = t == own_mate
    far = t == lax.rem(own_mate + 2, n_tp)
    inner = lax.div(f, half) == lax.div(t, 2)
    cross = pl.ds((1 - lax.div(f, half)) * half, half)
    every = pl.ds(0, n_fs)
    both = pl.ds(0, per)
    x = lax.rem(f, 2)
    z = lax.div(f, 2)

    third = rows // 48 * 16
    odd = rows - 2 * third
    few = experts // 3
    many = (experts - few) // 2
    wide = ((0, 0, 0, odd), (0, 1, odd, third), (0, 2, odd + third, third),
            (1, 0, 0, third), (1, 1, third, third), (1, 2, 2 * third, odd))
    slim = ((2, 0, 0, many), (2, 1, many, few), (2, 2, many + few, experts - many - few))

    def at(p, j):
        k, _, first, size = p
        if k < 2:
            return (k, j, pl.ds(first, size))
        return (k, pl.ds(first, size), pl.ds(pl.multiple_of(j * strip, strip), strip))

    def split(p, j, which):
        index = at(p, j)
        return index[:2] + (which,) + index[2:]

    def name(p):
        return 3 * p[0] + p[1]

    def on_stage(p, j, which):
        return stage.at[split(p, j, which)]

    def hop(p, j):
        return pltpu.make_async_remote_copy(
            src_ref=cast.at[split(p, j, both)], dst_ref=relay_buf.at[split(p, j, both)], send_sem=hop_send.at[name(p), j],
            recv_sem=hop_recv.at[name(p), j], device_id=(f, side), device_id_type=MESH)

    def straight(p, j, h):
        return pltpu.make_async_remote_copy(
            src_ref=cast.at[split(p, j, h)], dst_ref=on_stage(p, j, f),
            send_sem=own_send.at[name(p), j, h], recv_sem=land.at[name(p), j],
            device_id=(t * per + h, mate), device_id_type=MESH)

    def relayed(p, j, h):
        return pltpu.make_async_remote_copy(
            src_ref=relay_buf.at[split(p, j, h)], dst_ref=on_stage(p, j, f),
            send_sem=pass_send.at[name(p), j, h], recv_sem=land.at[name(p), j],
            device_id=(side * per + h, mate), device_id_type=MESH)

    def to_mate(p, j):
        return pltpu.make_async_remote_copy(
            src_ref=on_stage(p, j, every), dst_ref=on_stage(p, j, every), send_sem=core_send.at[name(p), j],
            recv_sem=land.at[name(p), j], device_id=(f, mate), device_id_type=MESH)

    def to_side(p, j):
        which = cross if p[1] == 2 else every
        return pltpu.make_async_remote_copy(
            src_ref=on_stage(p, j, which), dst_ref=on_stage(p, j, which), send_sem=side_send.at[name(p), j],
            recv_sem=land.at[name(p), j], device_id=(f, side), device_id_type=MESH)

    def landed(p, j):
        to_mate(p, j).wait_recv()

    def each(j, act):
        @pl.when((j >= 0) & (j < experts))
        def _():
            act(wide, j, j)

        if act is pushed_now:
            return

        @pl.when((j >= experts) & (j < chunks))
        def _():
            act(slim, j - experts, j)

    def reads(group, j, at_j):
        slot = lax.rem(at_j, 2)
        if group is wide:
            return [pltpu.make_async_copy(ref.at[j], raw.at[slot, k], fetch.at[slot, k])
                    for k, ref in enumerate((gate_in, up_in))]
        now = pl.ds(pl.multiple_of(j * strip, strip), strip)
        return [pltpu.make_async_copy(down_in.at[:, now], raw_down.at[slot], fetch_down.at[slot])]

    def ask(group, j, at_j):
        for copy in reads(group, j, at_j):
            copy.start()

    def rounded(group, j, at_j):
        slot = lax.rem(at_j, 2)
        each(at_j + 1, ask)
        for copy in reads(group, j, at_j):
            copy.wait()
        if group is wide:
            for k in range(2):
                for h in range(per):
                    here = raw[slot, k, :, h * unit:(h + 1) * unit]
                    cast[k, j, h] = (here * scale[:, :1]).astype(jnp.bfloat16)
        else:
            now = pl.ds(pl.multiple_of(j * strip, strip), strip)
            for h in range(per):
                cast[2, :, h, now, :] = raw_down[slot, :, :, h * unit:(h + 1) * unit].astype(jnp.bfloat16)

    def by_route(group, *routes):
        return [p for k in range(3) for r in routes for p in group if p[0] == k and p[1] == r]

    def push(group, j):
        for p in by_route(group, 2, 1):
            hop(p, j).start()
        for p in by_route(group, 0, 1):
            for h in range(per):
                straight(p, j, h).start()

        @pl.when(inner)
        def _():
            for p in by_route(group, 2):
                for h in range(per):
                    straight(p, j, h).start()

    def pushed_now(group, j, at_j):
        push([p for p in group if p[0] == 0], j)

    def pushed_later(group, j, at_j):
        push([p for p in group if p[0] > 0], j)

    def passed(group, j, at_j):
        for p in by_route(group, 2, 1):
            hop(p, j).wait_recv()
            for h in range(per):
                relayed(p, j, h).start()

    def spread(group, j, at_j):
        def out_of(first):
            for p in by_route(group, first, 1):
                landed(p, j)
                if p[1] != 1:
                    to_side(p, j).start()
                to_mate(p, j).start()

        @pl.when(near)
        def _():
            out_of(0)

        @pl.when(far)
        def _():
            out_of(2)

    fair = normed.shape[0] // NORM_STEPS

    def norm_rows(i):
        now = pl.ds(pl.multiple_of(i * fair, fair), fair)
        values = tokens[now, :].astype(jnp.float32)
        centered = values - jnp.mean(values, axis=1, keepdims=True)
        variance = jnp.mean(centered * centered, axis=1, keepdims=True)
        normed[now, :] = (centered * lax.rsqrt(variance + norm_eps)).astype(jnp.bfloat16)

    tall = normed.shape[0] // 2
    deep = n_fs * rows
    short = normed.shape[0] // n_fs
    breadth = n_fs * strip

    def fill_hidden(e):
        copies = [pltpu.make_async_copy(stage.at[k, e], held.at[k], load.at[k]) for k in range(2)]
        for copy in copies:
            copy.start()
        for copy in copies:
            copy.wait()

        def some_rows(i, carry):
            now = pl.ds(pl.multiple_of(i * tall, tall), tall)
            fed = normed[now, :]
            gate_act = jnp.dot(fed, held[0].reshape(deep, unit), preferred_element_type=jnp.float32)
            up_act = jnp.dot(fed, held[1].reshape(deep, unit), preferred_element_type=jnp.float32)
            lanes = lax.broadcasted_iota(jnp.int32, (tall, gates.shape[1]), 1)
            gate = jnp.sum(jnp.where(lanes == e, gates[now, :], 0.0), axis=1, keepdims=True)
            hidden = gate_act / (1.0 + jnp.exp(-gate_act)) * up_act * gate
            hid[e, now, :] = hidden.astype(jnp.bfloat16)
            return carry

        lax.fori_loop(0, 2, some_rows, 0)

    def pair(q):
        return pltpu.make_async_remote_copy(
            src_ref=leaving.at[q], dst_ref=arriving.at[q], send_sem=pair_send.at[q], recv_sem=pair_recv.at[q],
            device_id=(f + 1 - 2 * x, t), device_id_type=MESH)

    def merge(q):
        pair(q).wait_recv()
        now = pl.ds(pl.multiple_of(q * breadth, breadth), breadth)
        for ahead in range(zs):
            goal = lax.rem(z + ahead, zs)
            total = staying[q, goal] + arriving[q, goal].astype(jnp.float32)
            sums[ahead][:, now] = total.astype(jnp.bfloat16)

    def sum_strip(q):
        now = pl.ds(pl.multiple_of(q * strip, strip), strip)
        copy = pltpu.make_async_copy(stage.at[2, :, :, now], held_down, load_down)
        copy.start()

        @pl.when(q >= 1)
        def _():
            merge(q - 1)

        copy.wait()

        def some_rows(i, carry):
            now = pl.ds(pl.multiple_of(i * tall, tall), tall)
            acc = jnp.zeros((tall, breadth), jnp.float32)
            for e in range(experts):
                acc += lax.dot_general(
                    hid[e, now, :], held_down[e].reshape(breadth, unit), (((1,), (1,)), ((), ())),
                    preferred_element_type=jnp.float32)
            strip_sum[now, :] = acc
            return carry

        lax.fori_loop(0, 2, some_rows, 0)
        for goal in range(zs):
            theirs = pl.ds(pl.multiple_of((2 * goal + 1 - x) * short, short), short)
            leaving[q, goal] = strip_sum[theirs, :].astype(jnp.bfloat16)
        for goal in range(zs):
            mine = pl.ds(pl.multiple_of((2 * goal + x) * short, short), short)
            staying[q, goal] = strip_sum[mine, :]
        pair(q).start()

    def used(group, j, at_j):
        @pl.when(near)
        def _():
            for p in by_route(group, 2):
                landed(p, j)
                to_mate(p, j).start()

        @pl.when(far)
        def _():
            for p in by_route(group, 0):
                landed(p, j)
                to_mate(p, j).start()

        @pl.when(jnp.logical_not(near | far))
        def _():
            for p in group:
                landed(p, j)

        if group is wide:
            fill_hidden(j)
        else:
            sum_strip(j)

    def opened(j):
        each(j - 1, pushed_later)
        each(j, rounded)
        each(j, pushed_now)

    ask(wide, 0, 0)
    scale[...] = jnp.broadcast_to(gain[...], (128, rows)).T

    def early(j, carry):
        opened(j)
        return carry

    lax.fori_loop(0, LEAD + 1, early, 0)
    expert = lax.broadcasted_iota(jnp.int32, (128, ids.shape[1]), 0)
    chosen = sum(jnp.where(ids[c:c + 1, :] == expert, mix[c:c + 1, :], 0.0) for c in range(2))
    gates[...] = chosen.T

    def step(s, carry):
        opened(s + LEAD + 1)
        each(s, passed)

        @pl.when(s < NORM_STEPS)
        def _():
            norm_rows(s)

        each(s - LAG, spread)
        each(s - LAG - GAP, used)
        return carry

    lax.fori_loop(0, chunks + LAG + GAP, step, 0)
    merge(STRIPS - 1)

    def drain(group):
        def some(j, carry):
            for p in by_route(group, 1, 2):
                hop(p, j).wait_send()
                for h in range(per):
                    relayed(p, j, h).wait_send()
            for p in by_route(group, 0, 1):
                for h in range(per):
                    straight(p, j, h).wait_send()

            @pl.when(inner)
            def _():
                for p in by_route(group, 2):
                    for h in range(per):
                        straight(p, j, h).wait_send()

            @pl.when(near | far)
            def _():
                for p in group:
                    to_mate(p, j).wait_send()

            @pl.when(near)
            def _():
                for p in by_route(group, 0):
                    to_side(p, j).wait_send()

            @pl.when(far)
            def _():
                for p in by_route(group, 2):
                    to_side(p, j).wait_send()

            if group is slim:
                pair(j).wait_send()
            return carry

        return some

    lax.fori_loop(0, experts, drain(wide), 0)
    lax.fori_loop(0, STRIPS, drain(slim), 0)


def exchange(n_fs, n_tp, tokens, gain, ids, mix, weights):
    experts, rows, columns = weights[0].shape
    per = n_fs // n_tp
    unit = columns // per
    count, width = tokens.shape
    zs = n_fs // 2
    short = count // n_fs
    strip = rows // STRIPS
    longest = max(experts, STRIPS)
    serve = jax.ShapeDtypeStruct((3, experts, n_fs, rows, unit), jnp.bfloat16)
    relay = jax.ShapeDtypeStruct((3, experts, per, rows, unit), jnp.bfloat16)
    piece = jax.ShapeDtypeStruct((short, width), jnp.bfloat16)
    dma = pltpu.SemaphoreType.DMA
    vmem = pl.BlockSpec(memory_space=pltpu.VMEM)
    hbm = pl.BlockSpec(memory_space=pl.ANY)
    outs = pl.pallas_call(
        functools.partial(exchange_kernel, n_fs, n_tp),
        out_shape=(serve, relay) + (piece,) * zs,
        in_specs=[vmem] * 4 + [hbm] * 3,
        out_specs=[hbm] * 2 + [vmem] * zs,
        scratch_shapes=[
            pltpu.VMEM((rows, 128), jnp.float32),
            pltpu.VMEM((3, experts, per, rows, unit), jnp.bfloat16),
            pltpu.VMEM((2, 2, rows, columns), jnp.float32),
            pltpu.VMEM((2, experts, strip, columns), jnp.float32),
            pltpu.VMEM((count, width), jnp.bfloat16),
            pltpu.VMEM((count, 128), jnp.float32),
            pltpu.VMEM((experts, count, unit), jnp.bfloat16),
            pltpu.VMEM((2, n_fs, rows, unit), jnp.bfloat16),
            pltpu.VMEM((experts, n_fs, strip, unit), jnp.bfloat16),
            pltpu.VMEM((count, n_fs * strip), jnp.float32),
            pltpu.VMEM((STRIPS, zs, short, n_fs * strip), jnp.bfloat16),
            pltpu.VMEM((STRIPS, zs, short, n_fs * strip), jnp.float32),
            pltpu.VMEM((STRIPS, zs, short, n_fs * strip), jnp.bfloat16),
            dma((9, longest)),
            dma((9, longest)),
            dma((9, longest, per)),
            dma((9, longest, per)),
            dma((9, longest)),
            dma((9, longest)),
            dma((9, longest)),
            dma((2,)),
            dma,
            dma((2, 2)),
            dma((2,)),
            dma((STRIPS,)),
            dma((STRIPS,)),
        ],
        compiler_params=pltpu.CompilerParams(has_side_effects=True, vmem_limit_bytes=60 * 1024 * 1024),
    )(tokens, gain, ids, mix, *weights)
    return outs[0].reshape(3, experts, n_fs * rows, unit), outs[2:]


def copy_kernel(*refs):
    half = len(refs) // 2
    for source, target in zip(refs[:half], refs[half:]):
        target[...] = source[0]


def copied(staged):
    kinds, experts, deep, unit = staged.shape
    block = pl.BlockSpec((1, deep, unit), lambda e: (e, 0, 0))
    return pl.pallas_call(
        copy_kernel,
        grid=(experts,),
        out_shape=(jax.ShapeDtypeStruct(staged.shape[1:], staged.dtype),) * kinds,
        in_specs=[pl.BlockSpec((1, 1, deep, unit), functools.partial(lambda k, e: (k, e, 0, 0), k)) for k in range(kinds)],
        out_specs=[block] * kinds,
        cost_estimate=pl.CostEstimate(flops=0, bytes_accessed=4 * staged.size, transcendentals=0),
        compiler_params=pltpu.CompilerParams(vmem_limit_bytes=40 * 1024 * 1024),
    )(*(staged,) * kinds)


def sum_pieces(pieces, n_fs):
    zs = len(pieces)
    got = [pieces[0]]
    for ahead in range(1, zs):
        got.append(lax.ppermute(pieces[ahead], "fs", [(i, (i + 2 * ahead) % n_fs) for i in range(n_fs)]))
    summed = sum(g.astype(jnp.float32) for g in got).astype(jnp.bfloat16)
    short, width = summed.shape
    return summed.reshape(short, STRIPS, n_fs, -1).transpose(0, 2, 1, 3).reshape(short, width)


def collective_exchange(blocks):
    regrouped = [lax.all_to_all(b, "tp", split_axis=0, concat_axis=2, tiled=True) for b in blocks]
    unit_split = [lax.all_to_all(b, "fs", split_axis=2, concat_axis=1, tiled=True) for b in regrouped]
    return tuple(lax.all_gather(b, "tp", axis=0, tiled=True) for b in unit_split)


def expert_layer(normed, expert_gates, gate_serve, up_serve, down_serve):
    gate_act = jnp.einsum("rd,edf->ref", normed, gate_serve, preferred_element_type=jnp.float32)
    up_act = jnp.einsum("rd,edf->ref", normed, up_serve, preferred_element_type=jnp.float32)
    hidden = (jax.nn.silu(gate_act) * up_act * expert_gates[:, :, None]).astype(jnp.bfloat16)
    return jnp.einsum("ref,edf->rd", hidden, down_serve, preferred_element_type=jnp.float32).astype(jnp.bfloat16)


def sum_parts(parts):
    parts = lax.all_to_all(parts, "fs", split_axis=0, concat_axis=0, tiled=True)
    return jnp.sum(parts.astype(jnp.float32), axis=0)


def local(tokens, norm_gain, gate_weight, up_weight, down_weight, expert_ids, expert_mix):
    n_fs, n_tp = lax.axis_size("fs"), lax.axis_size("tp")
    width = tokens.shape[2]
    token_rows = tokens.reshape(-1, width)
    count = token_rows.shape[0]
    own_rows = count // n_fs
    route_ids = expert_ids.reshape(-1, 2)
    route_mix = expert_mix.reshape(-1, 2)
    experts, rows, columns = gate_weight.shape
    unit = columns * n_tp // n_fs
    cut = experts >= 3 and rows >= 48 and rows % (16 * STRIPS) == 0 and (rows // STRIPS * n_fs) % 128 == 0
    whole = count % (128 * NORM_STEPS // 2) == 0 and own_rows % 16 == 0 and n_fs % 2 == 0
    if n_tp == 4 and n_fs % n_tp == 0 and unit % 128 == 0 and cut and whole:
        staged, pieces = exchange(
            n_fs, n_tp, token_rows, norm_gain[None, :], route_ids.T, route_mix.T, (gate_weight, up_weight, down_weight))
        gate_serve, up_serve, down_serve = copied(staged)
        mixed = sum_pieces(pieces, n_fs)
    else:
        blocks = (
            (gate_weight * norm_gain[None, :, None]).astype(jnp.bfloat16),
            (up_weight * norm_gain[None, :, None]).astype(jnp.bfloat16),
            down_weight.astype(jnp.bfloat16),
        )
        values = token_rows.astype(jnp.float32)
        centered = values - jnp.mean(values, axis=1, keepdims=True)
        variance = jnp.mean(centered * centered, axis=1, keepdims=True)
        normed = (centered * lax.rsqrt(variance + norm_eps)).astype(jnp.bfloat16)
        expert_iota = jnp.arange(experts, dtype=jnp.int32)
        chosen = (route_ids[:, :, None] == expert_iota[None, None, :]).astype(jnp.float32)
        expert_gates = jnp.sum(chosen * route_mix[:, :, None], axis=1)
        gate_serve, up_serve, down_serve = collective_exchange(blocks)
        partial = expert_layer(normed, expert_gates, gate_serve, up_serve, down_serve)
        mixed = sum_parts(partial.reshape(n_fs, own_rows, width)).astype(jnp.bfloat16)
    return (gate_serve, up_serve, down_serve, mixed.reshape(own_rows, 1, width))


def solution(mesh):
    return jax.shard_map(
        local,
        mesh=mesh,
        in_specs=(
            P(None, "tp", None),
            P("fs"),
            P(None, "fs", "tp"),
            P(None, "fs", "tp"),
            P(None, "fs", "tp"),
            P(None, "tp", None),
            P(None, "tp", None),
        ),
        out_specs=(
            P(None, None, "fs"),
            P(None, None, "fs"),
            P(None, None, "fs"),
            P("fs", "tp", None),
        ),
        check_vma=False,
    )
```

time: 498 us -> 450 us (0.904)
  the two profiles are of different devices: /device:TPU:24 before, /device:TPU:11 now
where the time goes in v1:
time: 450 us; the launch traced here: 447 us
  Pallas kernels  438 us (97%)
  starting transfers between devices  4.5 us (1%)
    pallas_call x1, Pallas kernels, exchange(): pl.pallas_call(functools.partial(exchange_kernel, n_fs, n_tp), out_shape=...  406 us
    pallas_call x1, Pallas kernels, copied(): pl.pallas_call(copy_kernel, grid=(experts,), out_shape=(jax.ShapeDtypeStr...  32 us
  transfers between devices with their start and end apart: 3, of which 1 were waited for; matrix products, arithmetic and copies ran while one was open for 0% of the time, Pallas kernels for 7%

profile of v1, /device:TPU:11, one launch (start us, length us, event | category | flops | bytes accessed | tf_op | source)
XLA Modules:
  0.0 446.6 jit_solution(9228131445061276429)
XLA Ops:
  0.6 406.2 %shard_map.102 = (bf16[3,8,8,256,512]{4,3,2,1,0:T(8,128)(2,1)}, bf16[3,8,2,256,512]{4,3,2,1,0:T(8,128)(2,1)}, bf16[96,2048]{1,0:T(8,128)(2,1)}, bf16[96,2048]{1,...) custom-call(bf16[768,2048]{1,0:T(8,128)(2,1)} %bitcast.16, f32[1,256]{1,0:T(1,128)} %bitcast.21, ...), custom_call_target="tpu_custom_call" | custom-call | tf_op jit(solution)/shard_map/pallas_call | solution.py:373
  406.9 0.1 collective-permute-start
  406.9 3.1 collective-permute-start.1
  410.0 1.4 collective-permute-start.2
  411.4 0.0 copy-start
  411.4 32.0 %shard_map.103 = (bf16[8,2048,512]{2,1,0:T(8,128)(2,1)}, bf16[8,2048,512]{2,1,0:T(8,128)(2,1)}, bf16[8,2048,512]{2,1,0:T(8,128)(2,1)}) custom-call(bf16[3,8,2048,512]{3,2,1,0:T(8,128)(2,1)} %bitcast.13, bf16[3,8,2048,512]{3,2,1,0:T(8,128)(2,1)} %bitcast.14, bf16[3,8,2048,512]{3,2,1,0:T(8,128)(2,1)} %bitcast.15), custom_call_target="tpu_custom_call" | custom-call | bytes 100663296 | tf_op jit(solution)/shard_map/pallas_call | solution.py:420
  443.4 0.0 collective-permute-done
  443.4 0.0 collective-permute-done.1
  443.4 1.6 collective-permute-done.2
  445.0 0.0 copy-done
  445.0 0.2 add_convert_fusion
  445.3 0.3 copy.12
  445.6 1.0 copy.14
  (1 shorter events, 0.0 us)
Async XLA Ops:
  406.9 36.6 %collective-permute-start = (bf16[96,2048]{1,0:T(8,128)(2,1)}, bf16[96,2048]{1,0:T(8,128)(2,1)S(1)}, u32[]{:S(2)}, u32[]{:S(2)}) collective-permute-start(bf16[96,2048]{1,0:T(8,128)(2,1)} %get-tuple-element.17), channel_id=1, source_target_pairs={{0,8},{4,12},{8,16},{12,20},{16,24},{20,28},{24,0},{28,4},{1,9},{5... | collective-permute-start | bytes 1179656 | tf_op jit(solution)/shard_map/ppermute | solution.py:435
  406.9 36.5 %collective-permute-start.1 = (bf16[96,2048]{1,0:T(8,128)(2,1)}, bf16[96,2048]{1,0:T(8,128)(2,1)S(1)}, u32[]{:S(2)}, u32[]{:S(2)}) collective-permute-start(bf16[96,2048]{1,0:T(8,128)(2,1)} %get-tuple-element.18), channel_id=1, source_target_pairs={{0,16},{4,20},{8,24},{12,28},{16,0},{20,4},{24,8},{28,12},{1,17},{... | collective-permute-start | bytes 1179656 | tf_op jit(solution)/shard_map/ppermute | solution.py:435
  410.0 35.0 %collective-permute-start.2 = (bf16[96,2048]{1,0:T(8,128)(2,1)}, bf16[96,2048]{1,0:T(8,128)(2,1)S(1)}, u32[]{:S(2)}, u32[]{:S(2)}) collective-permute-start(bf16[96,2048]{1,0:T(8,128)(2,1)} %get-tuple-element.19), channel_id=1, source_target_pairs={{0,24},{4,28},{8,0},{12,4},{16,8},{20,12},{24,16},{28,20},{1,25},{... | collective-permute-start | bytes 1179656 | tf_op jit(solution)/shard_map/ppermute | solution.py:435
  411.4 33.6 %copy-start = (bf16[96,2048]{1,0:T(8,128)(2,1)S(1)}, bf16[96,2048]{1,0:T(8,128)(2,1)}, u32[]{:S(2)}) copy-start(bf16[96,2048]{1,0:T(8,128)(2,1)} %get-tuple-element.16) | copy-start | bytes 1179652

commit v2 on v1

--- a/solution.py
+++ b/solution.py
@@ -44,12 +44,11 @@
     x = lax.rem(f, 2)
     z = lax.div(f, 2)
 
-    third = rows // 48 * 16
-    odd = rows - 2 * third
+    mid = rows // 4
+    edge = (rows - mid) // 2
     few = experts // 3
     many = (experts - few) // 2
-    wide = ((0, 0, 0, odd), (0, 1, odd, third), (0, 2, odd + third, third),
-            (1, 0, 0, third), (1, 1, third, third), (1, 2, 2 * third, odd))
+    wide = tuple(p for k in range(2) for p in ((k, 0, 0, edge), (k, 1, edge, mid), (k, 2, edge + mid, edge)))
     slim = ((2, 0, 0, many), (2, 1, many, few), (2, 2, many + few, experts - many - few))
 
     def at(p, j):

time: 450 us -> 444 us (0.987)
  Pallas kernels: 438 us -> 432 us
    pallas_call x1, Pallas kernels: 406 us -> 400 us  [exchange(): pl.pallas_call(functools.partial(exchange_kernel, n_fs, n_tp), out_shape=...]
where the time goes in v2:
time: 444 us; the launch traced here: 441 us
  Pallas kernels  432 us (97%)
  starting transfers between devices  5.61 us (1%)
    pallas_call x1, Pallas kernels, exchange(): pl.pallas_call(functools.partial(exchange_kernel, n_fs, n_tp), out_shape=...  400 us
    pallas_call x1, Pallas kernels, copied(): pl.pallas_call(copy_kernel, grid=(experts,), out_shape=(jax.ShapeDtypeStr...  32 us
  transfers between devices with their start and end apart: 3, of which 1 were waited for; matrix products, arithmetic and copies ran while one was open for 0% of the time, Pallas kernels for 7%

profile of v2, /device:TPU:11, one launch (start us, length us, event | category | flops | bytes accessed | tf_op | source)
XLA Modules:
  0.0 441.5 jit_solution(5270478964069054675)
XLA Ops:
  0.6 400.0 %shard_map.102 = (bf16[3,8,8,256,512]{4,3,2,1,0:T(8,128)(2,1)}, bf16[3,8,2,256,512]{4,3,2,1,0:T(8,128)(2,1)}, bf16[96,2048]{1,0:T(8,128)(2,1)}, bf16[96,2048]{1,...) custom-call(bf16[768,2048]{1,0:T(8,128)(2,1)} %bitcast.16, f32[1,256]{1,0:T(1,128)} %bitcast.21, ...), custom_call_target="tpu_custom_call" | custom-call | tf_op jit(solution)/shard_map/pallas_call | solution.py:372
  400.7 0.1 collective-permute-start
  400.7 4.2 collective-permute-start.1
  404.9 1.4 collective-permute-start.2
  406.3 0.0 copy-start
  406.3 32.0 %shard_map.103 = (bf16[8,2048,512]{2,1,0:T(8,128)(2,1)}, bf16[8,2048,512]{2,1,0:T(8,128)(2,1)}, bf16[8,2048,512]{2,1,0:T(8,128)(2,1)}) custom-call(bf16[3,8,2048,512]{3,2,1,0:T(8,128)(2,1)} %bitcast.13, bf16[3,8,2048,512]{3,2,1,0:T(8,128)(2,1)} %bitcast.14, bf16[3,8,2048,512]{3,2,1,0:T(8,128)(2,1)} %bitcast.15), custom_call_target="tpu_custom_call" | custom-call | bytes 100663296 | tf_op jit(solution)/shard_map/pallas_call | solution.py:419
  438.3 0.0 collective-permute-done
  438.3 0.0 collective-permute-done.1
  438.3 1.6 collective-permute-done.2
  440.0 0.0 copy-done
  440.0 0.2 add_convert_fusion
  440.2 0.3 copy.12
  440.5 1.0 copy.14
  (1 shorter events, 0.0 us)
Async XLA Ops:
  400.7 37.7 %collective-permute-start = (bf16[96,2048]{1,0:T(8,128)(2,1)}, bf16[96,2048]{1,0:T(8,128)(2,1)S(1)}, u32[]{:S(2)}, u32[]{:S(2)}) collective-permute-start(bf16[96,2048]{1,0:T(8,128)(2,1)} %get-tuple-element.17), channel_id=1, source_target_pairs={{0,8},{4,12},{8,16},{12,20},{16,24},{20,28},{24,0},{28,4},{1,9},{5... | collective-permute-start | bytes 1179656 | tf_op jit(solution)/shard_map/ppermute | solution.py:434
  400.7 37.6 %collective-permute-start.1 = (bf16[96,2048]{1,0:T(8,128)(2,1)}, bf16[96,2048]{1,0:T(8,128)(2,1)S(1)}, u32[]{:S(2)}, u32[]{:S(2)}) collective-permute-start(bf16[96,2048]{1,0:T(8,128)(2,1)} %get-tuple-element.18), channel_id=1, source_target_pairs={{0,16},{4,20},{8,24},{12,28},{16,0},{20,4},{24,8},{28,12},{1,17},{... | collective-permute-start | bytes 1179656 | tf_op jit(solution)/shard_map/ppermute | solution.py:434
  404.9 35.1 %collective-permute-start.2 = (bf16[96,2048]{1,0:T(8,128)(2,1)}, bf16[96,2048]{1,0:T(8,128)(2,1)S(1)}, u32[]{:S(2)}, u32[]{:S(2)}) collective-permute-start(bf16[96,2048]{1,0:T(8,128)(2,1)} %get-tuple-element.19), channel_id=1, source_target_pairs={{0,24},{4,28},{8,0},{12,4},{16,8},{20,12},{24,16},{28,20},{1,25},{... | collective-permute-start | bytes 1179656 | tf_op jit(solution)/shard_map/ppermute | solution.py:434
  406.3 33.7 %copy-start = (bf16[96,2048]{1,0:T(8,128)(2,1)S(1)}, bf16[96,2048]{1,0:T(8,128)(2,1)}, u32[]{:S(2)}) copy-start(bf16[96,2048]{1,0:T(8,128)(2,1)} %get-tuple-element.16) | copy-start | bytes 1179652
